TPU v7x, 32 devices: a whole 2x2x4 slice. The times are simulated.
32 devices in a mesh: sp: 8 (over z, y), tp: 4 (over x, core).
Axes of the slice: x: 2, y: 2, z: 4, core: 2. Of those that a mesh axis runs over, the one named last changes fastest.
Arguments:
- inputs: bfloat16 [4096, 4096], P('sp', 'tp'), may hold values from -24 to 24
- length: int32 [1], replicated, may hold values from 2049 to 4096
- win_query: bfloat16 [4096, 1536], P(None, 'tp'), may hold values from -8 to 8
- win_key: bfloat16 [4096, 512], P(None, 'tp'), may hold values from -8 to 8
- win_value: bfloat16 [4096, 512], P(None, 'tp'), may hold values from -1.5 to 1.5
- sink_logit: float32 [24], P('tp'), may hold values from 4 to 8
- diff_query: bfloat16 [4096, 1024], P(None, 'tp'), may hold values from -8 to 8
- diff_key: bfloat16 [4096, 1024], P(None, 'tp'), may hold values from -8 to 8
- diff_value: bfloat16 [4096, 1024], P(None, 'tp'), may hold values from -0.09375 to 0.09375
- mix_lambda: float32 [16], P('tp'), may hold values from 0.3 to 0.8
- head_gain: float32 [64], replicated, may hold values from 0.1 to 1.9
- win_out: bfloat16 [1536, 4096], P('tp'), may hold values from -0.125 to 0.125
- diff_out: bfloat16 [1024, 4096], P('tp'), may hold values from -0.125 to 0.125
Outputs:
- merged_out: bfloat16 [4096, 4096], P(('sp', 'tp'))
All inputs are finite; a program needn't handle non-finite values.
Results may differ from a plain program's by a relative error of at most 0.015.
Values may be sent and summed in bfloat16 or wider, within the bound.
No kernel may reach another device: no remote copies, remote signals or barrier semaphores. Data moves between devices by JAX's collectives and lax.ppermute only.
A program may use at most 128 MiB of HBM per device.

v0:
```python
import jax
import jax.numpy as jnp
from jax import lax
from jax.sharding import PartitionSpec as P

HEAD = 64
DQK = 32
GROUP = 3
WINDOW = 128
epsilon = 1e-06
masked_score = -1e30


def extended(block, sides, width):
    for axis, dim in sides:
        count = lax.axis_size(axis)
        forward = [(i, i + 1) for i in range(count - 1)]
        backward = [(target, source) for source, target in forward]
        low = lax.ppermute(
            lax.slice_in_dim(block, block.shape[dim] - width, None, axis=dim), axis, forward
        )
        high = lax.ppermute(lax.slice_in_dim(block, 0, width, axis=dim), axis, backward)
        block = jnp.concatenate([low, block, high], axis=dim)
    return block


def window_part(win_q, win_k, win_v, sink_logit, live_count, offset):
    row_count = win_q.shape[0]
    kv_local = win_k.shape[1] // HEAD
    stacked = jnp.stack(
        (win_k.reshape(row_count, kv_local, HEAD), win_v.reshape(row_count, kv_local, HEAD)), axis=2
    )
    stacked = stacked.reshape(row_count, kv_local * 2 * HEAD)
    padded = extended(stacked, (("sp", 0),), WINDOW)
    padded = padded.reshape(row_count + 2 * WINDOW, kv_local, 2, HEAD)
    keys_win = padded[:, :, 0]
    values_win = padded[:, :, 1]
    queries = win_q.reshape(row_count, kv_local, GROUP, HEAD)
    sink_table = sink_logit.reshape(kv_local, GROUP)
    query_pos = offset + jnp.arange(row_count, dtype=jnp.int32)
    key_pos = offset - WINDOW + jnp.arange(row_count + 2 * WINDOW, dtype=jnp.int32)
    allowed = (
        (jnp.abs(query_pos[:, None] - key_pos[None, :]) <= WINDOW)
        & (key_pos[None, :] >= 0)
        & (key_pos[None, :] < live_count)
    )
    scores = jnp.einsum(
        "qhgd,khd->hgqk", queries, keys_win, preferred_element_type=jnp.float32
    ) * HEAD ** (-0.5)
    scores = jnp.where(allowed[None, None], scores, masked_score)
    row_max = jnp.maximum(jnp.max(scores, axis=-1), sink_table[:, :, None])
    exponent = jnp.where(allowed[None, None], jnp.exp(scores - row_max[..., None]), 0.0)
    denominator = jnp.sum(exponent, axis=-1) + jnp.exp(sink_table[:, :, None] - row_max)
    result = jnp.einsum(
        "hgqk,khd->qhgd",
        exponent.astype(jnp.bfloat16),
        values_win,
        preferred_element_type=jnp.float32,
    )
    result = result / jnp.transpose(denominator, (2, 0, 1))[..., None]
    result = jnp.where((query_pos < live_count)[:, None, None, None], result, 0.0)
    return result.reshape(row_count, kv_local * GROUP * HEAD).astype(jnp.bfloat16)


def attend(running, queries, key_part, value_part, live_count, block_total, query_step):
    key_length = key_part.shape[0]
    key_step = 4096

    def one_query_block(block_index, block_state):
        running_max, total_sum, weighted = block_state
        row_begin = block_index * query_step
        query_slab = lax.dynamic_slice_in_dim(queries, row_begin, query_step, 0)
        start_state = (
            lax.dynamic_slice_in_dim(running_max, row_begin, query_step, 2),
            lax.dynamic_slice_in_dim(total_sum, row_begin, query_step, 2),
            lax.dynamic_slice_in_dim(weighted, row_begin, query_step, 2),
        )

        def one_key_block(key_index, key_state):
            block_max, block_sum, block_weighted = key_state
            key_begin = key_index * key_step
            key_slab = lax.dynamic_slice_in_dim(key_part, key_begin, key_step, 0)
            value_slab = lax.dynamic_slice_in_dim(value_part, key_begin, key_step, 0)
            key_pos = key_begin + jnp.arange(key_step, dtype=jnp.int32)
            allowed = key_pos < live_count
            scores = jnp.einsum(
                "qhmd,khmd->hmqk", query_slab, key_slab, preferred_element_type=jnp.float32
            ) * DQK ** (-0.5)
            scores = jnp.where(allowed, scores, masked_score)
            new_max = jnp.maximum(block_max, jnp.max(scores, axis=-1))
            rescale = jnp.exp(block_max - new_max)
            exponent = jnp.where(allowed, jnp.exp(scores - new_max[..., None]), 0.0)
            new_total = block_sum * rescale + jnp.sum(exponent, axis=-1)
            new_weighted = block_weighted * rescale[..., None] + jnp.einsum(
                "hmqk,khd->hmqd",
                exponent.astype(jnp.bfloat16),
                value_slab,
                preferred_element_type=jnp.float32,
            )
            return (new_max, new_total, new_weighted)

        final_state = lax.fori_loop(0, key_length // key_step, one_key_block, start_state)
        return (
            lax.dynamic_update_slice_in_dim(running_max, final_state[0], row_begin, 2),
            lax.dynamic_update_slice_in_dim(total_sum, final_state[1], row_begin, 2),
            lax.dynamic_update_slice_in_dim(weighted, final_state[2], row_begin, 2),
        )

    return lax.fori_loop(0, block_total, one_query_block, running)


def diff_part(diff_q, diff_k, diff_v, mix_lambda, head_gain, live_count, offset):
    row_count = diff_q.shape[0]
    heads_local = mix_lambda.shape[0]
    query_step = 128
    positions = offset + jnp.arange(row_count, dtype=jnp.int32)
    live_rows = jnp.sum((positions < live_count).astype(jnp.int32))
    block_total = (live_rows + query_step - 1) // query_step
    queries = diff_q.reshape(row_count, heads_local, 2, DQK)
    zero_state = (
        jnp.full((heads_local, 2, row_count), masked_score, jnp.float32),
        jnp.zeros((heads_local, 2, row_count), jnp.float32),
        jnp.zeros((heads_local, 2, row_count, HEAD), jnp.float32),
    )
    key_part = lax.all_gather(diff_k, "sp", axis=0, tiled=True).reshape(-1, heads_local, 2, DQK)
    value_part = lax.all_gather(diff_v, "sp", axis=0, tiled=True).reshape(-1, heads_local, HEAD)
    running = lax.cond(
        jnp.int32(0) < live_count,
        lambda inner_state: attend(
            inner_state, queries, key_part, value_part, live_count, block_total, query_step
        ),
        lambda inner_state: inner_state,
        zero_state,
    )
    total_sum = running[1]
    safe_total = jnp.where(total_sum > 0.0, total_sum, 1.0)
    map_rows = running[2] / safe_total[..., None]
    mixed_rows = map_rows[:, 0] - mix_lambda[:, None, None] * map_rows[:, 1]
    normed = (
        mixed_rows
        * lax.rsqrt(jnp.mean(mixed_rows * mixed_rows, axis=-1, keepdims=True) + epsilon)
        * head_gain
    )
    normed = jnp.where((positions < live_count)[None, :, None], normed, 0.0)
    result = (
        jnp.transpose(normed, (1, 0, 2)).reshape(row_count, heads_local * HEAD).astype(jnp.bfloat16)
    )
    return result


def body(
    inputs,
    length,
    win_query,
    win_key,
    win_value,
    sink_logit,
    diff_query,
    diff_key,
    diff_value,
    mix_lambda,
    head_gain,
    win_out,
    diff_out,
):
    row_count = inputs.shape[0]
    live_count = length[0]
    weights = (win_query, win_key, win_value, diff_query, diff_key, diff_value)
    segment = lax.all_gather(inputs, "tp", axis=1, tiled=True)
    summed = tuple(
        (jnp.dot(segment, weight, preferred_element_type=jnp.float32) for weight in weights)
    )
    win_q, win_k, win_v, diff_q, diff_k, diff_v = [total.astype(jnp.bfloat16) for total in summed]
    offset = lax.axis_index("sp") * row_count
    win_rows = window_part(win_q, win_k, win_v, sink_logit, live_count, offset)
    diff_rows = diff_part(diff_q, diff_k, diff_v, mix_lambda, head_gain, live_count, offset)
    partial_value = jnp.dot(win_rows, win_out, preferred_element_type=jnp.float32)
    return lax.psum_scatter(
        (partial_value + jnp.dot(diff_rows, diff_out, preferred_element_type=jnp.float32)).astype(
            jnp.bfloat16
        ),
        "tp",
        scatter_dimension=0,
        tiled=True,
    )


def solution(mesh):
    placed = (
        P("sp", "tp"),
        P(),
        P(None, "tp"),
        P(None, "tp"),
        P(None, "tp"),
        P("tp"),
        P(None, "tp"),
        P(None, "tp"),
        P(None, "tp"),
        P("tp"),
        P(),
        P("tp", None),
        P("tp", None),
    )
    return jax.shard_map(
        body, mesh=mesh, in_specs=placed, out_specs=P(("sp", "tp"), None), check_vma=False
    )
```

profile of v0, /device:TPU:0, one launch (start us, length us, event | category | flops | bytes accessed | tf_op | source)
XLA Modules:
  0.0 299.4 jit_solution(1611999572940378291)
XLA Ops:
  7.3 38.8 %all-gather.4.cloned.1.call-done = bf16[512,4096]{1,0:T(8,128)(2,1)} async-done(((bf16[512,1024]{1,0:T(8,128)(2,1)}), bf16[512,4096]{1,0:T(8,128)(2,1)}) %all-gather.4.cloned.1.call-update) | async-done | bytes 4194320 | tf_op jit(solution)/shard_map/all_gather | solution.py:169
  46.1 4.8 %convolution_convert_fusion.1 = bf16[512,256]{1,0:T(8,128)(2,1)} fusion(bf16[512,4096]{1,0:T(8,128)(2,1)} %all-gather.4.cloned.1.call-done, bf16[4096,256]{1,0:T(8,128)(2,1)} %param.25), kind=kOutput, calls=%fused_computation.34 | convolution fusion | flops 1073872896 | bytes 6553600 | tf_op jit(solution)/shard_map/dot_general | solution.py:171
  52.6 4.4 %convolution_convert_fusion.4 = bf16[512,128]{0,1:T(8,128)(2,1)S(1)} fusion(bf16[512,4096]{1,0:T(8,128)(2,1)} %all-gather.4.cloned.1.call-done, bf16[4096,128]{1,0:T(8,128)(2,1)} %param.21), kind=kOutput, calls=%fused_computation.37 | convolution fusion | flops 536936448 | bytes 5373952 | tf_op jit(solution)/shard_map/dot_general | solution.py:171
  57.0 1.5 convolution_convert_fusion.5
  61.8 5.2 %collective-permute-start = (bf16[128,256]{0,1:T(8,128)(2,1)}, bf16[128,256]{0,1:T(8,128)(2,1)}, u32[]{:S(2)}, u32[]{:S(2)}) collective-permute-start(bf16[128,256]{0,1:T(8,128)(2,1)} %bitcast.8), channel_id=1, source_target_pairs={{0,4},{4,8},{8,12},{12,16},{16,20},{20,24},{24,28},{1,5},{5,9},{9,... | collective-permute-start | bytes 196616 | tf_op jit(solution)/shard_map/ppermute | solution.py:19
  67.0 2.0 convolution_convert_fusion.2
  69.2 5.2 %convolution_convert_fusion = bf16[512,384]{0,1:T(8,128)(2,1)S(1)} fusion(bf16[512,4096]{1,0:T(8,128)(2,1)} %all-gather.4.cloned.1.call-done, bf16[4096,384]{1,0:T(8,128)(2,1)} %param.19), kind=kOutput, calls=%fused_computation.33 | convolution fusion | flops 1610809344 | bytes 7733248 | tf_op jit(solution)/shard_map/dot_general | solution.py:171
  74.4 2.0 convolution_convert_fusion.3
  77.3 1.7 fusion.23
  79.1 2.3 fusion.24
  81.4 2.7 fusion.40
  84.1 5.6 %fusion.52 = f32[512,4096]{1,0:T(8,128)} fusion(bf16[512,384]{0,1:T(8,128)(2,1)S(1)} %bitcast.123, bf16[384,4096]{1,0:T(8,128)(2,1)S(1)} %copy-done), kind=kOutput, calls=%fused_computation.68 | convolution fusion | flops 1610612736 | bytes 11927552 | tf_op jit(solution)/shard_map/dot_general | solution.py:177
  89.7 11.3 %all-gather.8.cloned.1.call-done = bf16[4096,256]{1,0:T(8,128)(2,1)} async-done(((bf16[512,256]{1,0:T(8,128)(2,1)}), bf16[4096,256]{1,0:T(8,128)(2,1)}) %all-gather.8.cloned.1.call-update) | async-done | bytes 2097168 | tf_op jit(solution)/shard_map/all_gather | solution.py:126
  101.0 49.8 %all-gather.6.cloned.1.call-done = bf16[4096,256]{1,0:T(8,128)(2,1)} async-done(((bf16[512,256]{1,0:T(8,128)(2,1)}), bf16[4096,256]{1,0:T(8,128)(2,1)}) %all-gather.6.cloned.1.call-update) | async-done | bytes 2097168 | tf_op jit(solution)/shard_map/all_gather | solution.py:125
  150.8 89.2 %conditional.1 = (f32[4,2,512]{2,1,0:T(2,128)}, f32[4,2,512,64]{2,3,1,0:T(8,128)}) conditional(s32[]{:T(128)} %convert_element_type.55, () %tuple.34, (s32[512]{0:T(512)S(1)}, bf16[512,256]{1,0:T(8,128)(2,1)S(1)}, bf16[4096,256]{1,0:T(8,128)(2,1)}, bf16[4096,256]{1,0:T(8,128)(2,1)}, s32[]{:T(128)}, /*index=5*/s32[]{:T(128)}) %tuple.79), branch_computations={%region_3.4_spmd, %region_4.9_spmd.clone} | conditional | flops 859970048 | bytes 132364824 | solution.py:127
  152.3 4.1 %copy.34 = bf16[4096,256]{0,1:T(8,128)(2,1)} copy(bf16[4096,256]{1,0:T(8,128)(2,1)} %get-tuple-element.250) | data formatting | bytes 4194304 | tf_op jit(solution)/shard_map
  156.4 2.9 copy.33
  161.0 79.0 %while.37 = (s32[]{:T(128)}, f32[4,2,512]{2,1,0:T(2,128)S(1)}, f32[4,2,512]{2,1,0:T(2,128)}, f32[4,2,512,64]{2,3,1,0:T(8,128)}, s32[]{:T(128)}, /*index=5*/s32[]...) while((s32[]{:T(128)}, f32[4,2,512]{2,1,0:T(2,128)S(1)}, ...), condition=%wide.region_8.8_spmd, body=%wide.region_5.7_spmd.sunk | while | flops 859969536 | bytes 122368224 | solution.py:109
  161.7 2.7 fusion.82
  164.5 4.9 %fusion.83 = f32[4,2,128]{2,1,0:T(2,128)S(1)} fusion(f32[4,2,128,4096]{3,2,1,0:T(8,128)S(1)} %get-tuple-element.357, f32[4,2,128]{2,1,0:T(2,128)S(1)} %get-tuple-element.358, pred[4096]{0:T(1024)(128)(4,1)S(1)} %iota_compare_fusion.2), kind=kLoop, calls=%fused_computation.4.clone.1 | loop fusion | flops 20970496 | bytes 16789504 | tf_op jit(solution)/shard_map/cond/branch_1_fun/while/body/while/body/eval_jaxpr/reduce_sum | solution.py:93
  171.5 9.3 %fusion.84 = f32[4,2,512,64]{2,3,1,0:T(8,128)} fusion(f32[4,2,512,64]{2,3,1,0:T(8,128)} %get-tuple-element.377, s32[]{:T(128)S(6)} %select_n.128, bf16[4096,4,64]{0,2,1:T(8,128)(2,1)} %get-tuple-element.395, f32[4,2,128,4096]{3,2,1,0:T(8,128)} %copy-done.2, f32[4,2,128]{2,1,0:T(2,128)S(1)} %get-tuple-element.358, ...), kind=kOutput, calls=%fused_computation.9.clone.1 | convolution fusion | flops 557973504 | bytes 19410948 | tf_op jit(solution)/shard_map/cond/branch_1_fun/while/body/while/body/eval_jaxpr/hmqk,khd->hmqd/dot_general | solution.py:94
  181.5 2.7 fusion.82
  184.2 4.9 %fusion.83 = f32[4,2,128]{2,1,0:T(2,128)S(1)} fusion(f32[4,2,128,4096]{3,2,1,0:T(8,128)S(1)} %get-tuple-element.357, f32[4,2,128]{2,1,0:T(2,128)S(1)} %get-tuple-element.358, pred[4096]{0:T(1024)(128)(4,1)S(1)} %iota_compare_fusion.2), kind=kLoop, calls=%fused_computation.4.clone.1 | loop fusion | flops 20970496 | bytes 16789504 | tf_op jit(solution)/shard_map/cond/branch_1_fun/while/body/while/body/eval_jaxpr/reduce_sum | solution.py:93
  191.2 9.3 %fusion.84 = f32[4,2,512,64]{2,3,1,0:T(8,128)} fusion(f32[4,2,512,64]{2,3,1,0:T(8,128)} %get-tuple-element.377, s32[]{:T(128)S(6)} %select_n.128, bf16[4096,4,64]{0,2,1:T(8,128)(2,1)} %get-tuple-element.395, f32[4,2,128,4096]{3,2,1,0:T(8,128)} %copy-done.2, f32[4,2,128]{2,1,0:T(2,128)S(1)} %get-tuple-element.358, ...), kind=kOutput, calls=%fused_computation.9.clone.1 | convolution fusion | flops 557973504 | bytes 19410948 | tf_op jit(solution)/shard_map/cond/branch_1_fun/while/body/while/body/eval_jaxpr/hmqk,khd->hmqd/dot_general | solution.py:94
  201.2 2.7 fusion.82
  204.0 4.9 %fusion.83 = f32[4,2,128]{2,1,0:T(2,128)S(1)} fusion(f32[4,2,128,4096]{3,2,1,0:T(8,128)S(1)} %get-tuple-element.357, f32[4,2,128]{2,1,0:T(2,128)S(1)} %get-tuple-element.358, pred[4096]{0:T(1024)(128)(4,1)S(1)} %iota_compare_fusion.2), kind=kLoop, calls=%fused_computation.4.clone.1 | loop fusion | flops 20970496 | bytes 16789504 | tf_op jit(solution)/shard_map/cond/branch_1_fun/while/body/while/body/eval_jaxpr/reduce_sum | solution.py:93
  211.0 9.3 %fusion.84 = f32[4,2,512,64]{2,3,1,0:T(8,128)} fusion(f32[4,2,512,64]{2,3,1,0:T(8,128)} %get-tuple-element.377, s32[]{:T(128)S(6)} %select_n.128, bf16[4096,4,64]{0,2,1:T(8,128)(2,1)} %get-tuple-element.395, f32[4,2,128,4096]{3,2,1,0:T(8,128)} %copy-done.2, f32[4,2,128]{2,1,0:T(2,128)S(1)} %get-tuple-element.358, ...), kind=kOutput, calls=%fused_computation.9.clone.1 | convolution fusion | flops 557973504 | bytes 19410948 | tf_op jit(solution)/shard_map/cond/branch_1_fun/while/body/while/body/eval_jaxpr/hmqk,khd->hmqd/dot_general | solution.py:94
  221.0 2.7 fusion.82
  223.7 4.9 %fusion.83 = f32[4,2,128]{2,1,0:T(2,128)S(1)} fusion(f32[4,2,128,4096]{3,2,1,0:T(8,128)S(1)} %get-tuple-element.357, f32[4,2,128]{2,1,0:T(2,128)S(1)} %get-tuple-element.358, pred[4096]{0:T(1024)(128)(4,1)S(1)} %iota_compare_fusion.2), kind=kLoop, calls=%fused_computation.4.clone.1 | loop fusion | flops 20970496 | bytes 16789504 | tf_op jit(solution)/shard_map/cond/branch_1_fun/while/body/while/body/eval_jaxpr/reduce_sum | solution.py:93
  230.7 9.3 %fusion.84 = f32[4,2,512,64]{2,3,1,0:T(8,128)} fusion(f32[4,2,512,64]{2,3,1,0:T(8,128)} %get-tuple-element.377, s32[]{:T(128)S(6)} %select_n.128, bf16[4096,4,64]{0,2,1:T(8,128)(2,1)} %get-tuple-element.395, f32[4,2,128,4096]{3,2,1,0:T(8,128)} %copy-done.2, f32[4,2,128]{2,1,0:T(2,128)S(1)} %get-tuple-element.358, ...), kind=kOutput, calls=%fused_computation.9.clone.1 | convolution fusion | flops 557973504 | bytes 19410948 | tf_op jit(solution)/shard_map/cond/branch_1_fun/while/body/while/body/eval_jaxpr/hmqk,khd->hmqd/dot_general | solution.py:94
  242.7 6.8 %add_convert_fusion = bf16[512,4096]{1,0:T(8,128)(2,1)} fusion(f32[512,4096]{1,0:T(8,128)} %fusion.52, bf16[512,256]{0,1:T(8,128)(2,1)S(1)} %bitcast.122, bf16[256,4096]{1,0:T(8,128)(2,1)S(1)} %copy-done.5), kind=kOutput, calls=%fused_computation.23 | convolution fusion | flops 1077936128 | bytes 14942208 | tf_op jit(solution)/shard_map/dot_general | solution.py:179
  249.6 43.2 %reduce-scatter.2.cloned.1.call-done = bf16[128,4096]{1,0:T(8,128)(2,1)} async-done(((bf16[512,4096]{1,0:T(8,128)(2,1)}), bf16[128,4096]{1,0:T(8,128)(2,1)}) %reduce-scatter.2.cloned.1.call-update) | async-done | bytes 1048592 | tf_op jit(solution)/shard_map/reduce_scatter | solution.py:178
  (93 shorter events, 22.6 us)
Async XLA Ops:
  6.5 77.6 %copy-start = (bf16[384,4096]{1,0:T(8,128)(2,1)S(1)}, bf16[384,4096]{1,0:T(8,128)(2,1)}, u32[]{:S(2)}) copy-start(bf16[384,4096]{1,0:T(8,128)(2,1)} %param.28) | copy-start | bytes 9437188
  6.5 39.6 %all-gather.4.cloned.1.call-start = ((), (), s32[]{:S(2)}) async-start(), calls=%async_computation.1 | async-start | bytes 5242880 | tf_op jit(solution)/shard_map/all_gather | solution.py:169
  7.3 44.4 %copy-start.16 = (f32[6]{0:T(128)S(1)}, f32[6]{0:T(128)}, u32[]{:S(2)}) copy-start(f32[6]{0:T(128)} %param.22) | copy-start | bytes 76
  7.3 93.7 %all-gather.8.cloned.1.call-start = ((), (), s32[]{:S(2)}) async-start(), calls=%async_computation.3 | async-start | bytes 2359296 | tf_op jit(solution)/shard_map/all_gather | solution.py:126
  51.0 99.8 %all-gather.6.cloned.1.call-start = ((), (), s32[]{:S(2)}) async-start(), calls=%async_computation.2 | async-start | bytes 2359296 | tf_op jit(solution)/shard_map/all_gather | solution.py:125
  51.8 5.2 %copy-start.3 = (bf16[512,4096]{1,0:T(8,128)(2,1)S(1)}, bf16[512,4096]{1,0:T(8,128)(2,1)}, u32[]{:S(2)}) copy-start(bf16[512,4096]{1,0:T(8,128)(2,1)} %all-gather.4.cloned.1.call-done) | copy-start | bytes 12582916
  51.8 5.2 %copy-start.10 = (bf16[4096,128]{1,0:T(8,128)(2,1)S(1)}, bf16[4096,128]{1,0:T(8,128)(2,1)}, u32[]{:S(2)}) copy-start(bf16[4096,128]{1,0:T(8,128)(2,1)} %param.20) | copy-start | bytes 3145732
  57.0 1.5 copy-start.6
  57.0 9.9 %copy-start.14 = (bf16[4096,256]{1,0:T(8,128)(2,1)S(1)}, bf16[4096,256]{1,0:T(8,128)(2,1)}, u32[]{:S(2)}) copy-start(bf16[4096,256]{1,0:T(8,128)(2,1)} %param.24) | copy-start | bytes 6291460
  58.6 0.7 copy-start.8
  60.5 15.9 %collective-permute-start.1 = (bf16[128,256]{0,1:T(8,128)(2,1)}, bf16[128,256]{0,1:T(8,128)(2,1)}, u32[]{:S(2)}, u32[]{:S(2)}) collective-permute-start(bf16[128,256]{0,1:T(8,128)(2,1)} %bitcast.10), channel_id=1, source_target_pairs={{4,0},{8,4},{12,8},{16,12},{20,16},{24,20},{28,24},{5,1},{9,5},{13... | collective-permute-start | bytes 196616 | tf_op jit(solution)/shard_map/ppermute | solution.py:22
  61.8 14.6 %collective-permute-start = (bf16[128,256]{0,1:T(8,128)(2,1)}, bf16[128,256]{0,1:T(8,128)(2,1)}, u32[]{:S(2)}, u32[]{:S(2)}) collective-permute-start(bf16[128,256]{0,1:T(8,128)(2,1)} %bitcast.8), channel_id=1, source_target_pairs={{0,4},{4,8},{8,12},{12,16},{16,20},{20,24},{24,28},{1,5},{5,9},{9,... | collective-permute-start | bytes 196616 | tf_op jit(solution)/shard_map/ppermute | solution.py:19
  69.0 223.9 %reduce-scatter.2.cloned.1.call-start = ((), (), s32[]{:S(2)}) async-start(), calls=%async_computation.4 | async-start | bytes 5242880 | tf_op jit(solution)/shard_map/reduce_scatter | solution.py:178
  69.2 5.2 %copy-start.4 = (bf16[512,4096]{1,0:T(8,128)(2,1)S(1)}, bf16[512,4096]{1,0:T(8,128)(2,1)}, u32[]{:S(2)}) copy-start(bf16[512,4096]{1,0:T(8,128)(2,1)} %all-gather.4.cloned.1.call-done) | copy-start | bytes 12582916
  69.2 5.2 %copy-start.15 = (bf16[4096,256]{1,0:T(8,128)(2,1)S(1)}, bf16[4096,256]{1,0:T(8,128)(2,1)}, u32[]{:S(2)}) copy-start(bf16[4096,256]{1,0:T(8,128)(2,1)} %param.23) | copy-start | bytes 6291460
  74.4 2.0 copy-start.7
  74.4 2.0 copy-start.9
  84.1 66.7 %copy-start.11 = (bf16[512,256]{1,0:T(8,128)(2,1)S(1)}, bf16[512,256]{1,0:T(8,128)(2,1)}, u32[]{:S(2)}) copy-start(bf16[512,256]{1,0:T(8,128)(2,1)} %convolution_convert_fusion.3) | copy-start | bytes 786436
  150.8 91.5 %copy-start.12 = (f32[4]{0:T(128)S(1)}, f32[4]{0:T(128)}, u32[]{:S(2)}) copy-start(f32[4]{0:T(128)} %param.26) | copy-start | bytes 52
  150.8 91.7 %copy-start.13 = (f32[64]{0:T(128)S(1)}, f32[64]{0:T(128)}, u32[]{:S(2)}) copy-start(f32[64]{0:T(128)} %param.27) | copy-start | bytes 772
  164.4 5.7 %copy-start.2 = (f32[4,2,128,4096]{3,2,1,0:T(8,128)}, f32[4,2,128,4096]{3,2,1,0:T(8,128)S(1)}, u32[]{:S(2)}) copy-start(f32[4,2,128,4096]{3,2,1,0:T(8,128)S(1)} %get-tuple-element.357) | copy-start | bytes 50331652 | tf_op jit(solution)/shard_map/cond/branch_1_fun/while
  184.2 5.7 %copy-start.2 = (f32[4,2,128,4096]{3,2,1,0:T(8,128)}, f32[4,2,128,4096]{3,2,1,0:T(8,128)S(1)}, u32[]{:S(2)}) copy-start(f32[4,2,128,4096]{3,2,1,0:T(8,128)S(1)} %get-tuple-element.357) | copy-start | bytes 50331652 | tf_op jit(solution)/shard_map/cond/branch_1_fun/while
  204.0 5.7 %copy-start.2 = (f32[4,2,128,4096]{3,2,1,0:T(8,128)}, f32[4,2,128,4096]{3,2,1,0:T(8,128)S(1)}, u32[]{:S(2)}) copy-start(f32[4,2,128,4096]{3,2,1,0:T(8,128)S(1)} %get-tuple-element.357) | copy-start | bytes 50331652 | tf_op jit(solution)/shard_map/cond/branch_1_fun/while
  223.7 5.7 %copy-start.2 = (f32[4,2,128,4096]{3,2,1,0:T(8,128)}, f32[4,2,128,4096]{3,2,1,0:T(8,128)S(1)}, u32[]{:S(2)}) copy-start(f32[4,2,128,4096]{3,2,1,0:T(8,128)S(1)} %get-tuple-element.357) | copy-start | bytes 50331652 | tf_op jit(solution)/shard_map/cond/branch_1_fun/while
  240.1 2.7 copy-start.5
  242.7 50.1 %copy-start.1 = (bf16[384,4096]{1,0:T(8,128)(2,1)S(1)}, bf16[384,4096]{1,0:T(8,128)(2,1)}, u32[]{:S(2)}) copy-start(bf16[384,4096]{1,0:T(8,128)(2,1)} %param.28) | copy-start | bytes 9437188
Sparse Core Ops, SparseCore 0:
  8.9 37.1 all-gather.3
  51.1 49.8 all-gather.7
  103.1 47.6 all-gather.5
  249.7 43.0 reduce-scatter.1
where the time goes:
time: 300 us; the launch traced here: 299 us
  waiting for transfers between devices  144 us (48%)
  matrix products  84.8 us (28%)
  other arithmetic  34.7 us (12%)
  local copies, waits for them, and re-layouts  14.3 us (5%)
  between operations  14.1 us (5%)
  starting transfers between devices  6.77 us (2%)
    all_gather x1, waiting for transfers between devices, diff_part(): lax.all_gather(diff_k, 'sp', axis=0, tiled=True)  49.8 us
    reduce_scatter x1, waiting for transfers between devices, body(): lax.psum_scatter((partial_value + jnp.dot(diff_rows, diff_out, preferred_...  43.2 us
    all_gather x1, waiting for transfers between devices, body(): segment = lax.all_gather(inputs, 'tp', axis=1, tiled=True)  38.8 us
    dot_general x4, matrix products, one_key_block(): jnp.einsum('hmqk,khd->hmqd', exponent.astype(jnp.bfloat16), value_slab, p...  37.3 us
    dot_general x6, matrix products, body(): jnp.dot(segment, weight, preferred_element_type=jnp.float32)  19.8 us
    reduce_sum x4, other arithmetic, one_key_block(): new_total = block_sum * rescale + jnp.sum(exponent, axis=-1)  19.5 us
    all_gather x1, waiting for transfers between devices, diff_part(): lax.all_gather(diff_v, 'sp', axis=0, tiled=True)  11.3 us
    dot_general x4, matrix products, one_key_block(): jnp.einsum('qhmd,khmd->hmqk', query_slab, key_slab, preferred_element_typ...  11 us
  transfers between devices with their start and end apart: 6, of which 4 were waited for; matrix products, arithmetic and copies ran while one was open for 10% of the time, Pallas kernels for 0%

commit v1 on v0

--- a/solution.py
+++ b/solution.py
@@ -166,7 +166,7 @@
     row_count = inputs.shape[0]
     live_count = length[0]
     weights = (win_query, win_key, win_value, diff_query, diff_key, diff_value)
-    segment = lax.all_gather(inputs, "tp", axis=1, tiled=True)
+    segment = jnp.concatenate(lax.all_gather(inputs, "tp"), axis=1)
     summed = tuple(
         (jnp.dot(segment, weight, preferred_element_type=jnp.float32) for weight in weights)
     )

time: 300 us -> 306 us (1.020)
  local copies, waits for them, and re-layouts: 14.3 us -> 20.5 us
    reshape x0 -> x1, local copies, waits for them, and re-layouts: none -> 6.2 us  [body(): segment = jnp.concatenate(lax.all_gather(inputs, 'tp'), axis=1)]
  transfers between devices with their start and end apart: 6 -> 6, of which waited for: 4 -> 4; matrix products, arithmetic and copies ran while one was open for 10% -> 11% of each run, Pallas kernels for 0% -> 0%
where the time goes in v1:
time: 306 us
  waiting for transfers between devices  142 us (46%)
  matrix products  87.1 us (28%)
  other arithmetic  34.6 us (11%)
  local copies, waits for them, and re-layouts  20.5 us (7%)
  between operations  14 us (5%)
  starting transfers between devices  6.75 us (2%)
    all_gather x1, waiting for transfers between devices, diff_part(): lax.all_gather(diff_k, 'sp', axis=0, tiled=True)  49.8 us
    reduce_scatter x1, waiting for transfers between devices, body(): lax.psum_scatter((partial_value + jnp.dot(diff_rows, diff_out, preferred_...  43.2 us
    all_gather x1, waiting for transfers between devices, body(): segment = jnp.concatenate(lax.all_gather(inputs, 'tp'), axis=1)  38.8 us
    dot_general x4, matrix products, one_key_block(): jnp.einsum('hmqk,khd->hmqd', exponent.astype(jnp.bfloat16), value_slab, p...  37.3 us
    dot_general x6, matrix products, body(): jnp.dot(segment, weight, preferred_element_type=jnp.float32)  22.1 us
    reduce_sum x4, other arithmetic, one_key_block(): new_total = block_sum * rescale + jnp.sum(exponent, axis=-1)  19.5 us
    dot_general x4, matrix products, one_key_block(): jnp.einsum('qhmd,khmd->hmqk', query_slab, key_slab, preferred_element_typ...  11 us
    all_gather x1, waiting for transfers between devices, diff_part(): lax.all_gather(diff_v, 'sp', axis=0, tiled=True)  9.35 us
  transfers between devices with their start and end apart: 6, of which 4 were waited for; matrix products, arithmetic and copies ran while one was open for 11% of the time, Pallas kernels for 0%

profile of v1, /device:TPU:0, one launch (start us, length us, event | category | flops | bytes accessed | tf_op | source)
XLA Modules:
  0.0 305.7 jit_solution(2350559141903219995)
XLA Ops:
  7.3 38.8 %all-gather.9.cloned.1.call-done = bf16[2048,1024]{1,0:T(8,128)(2,1)} async-done(((bf16[512,1024]{1,0:T(8,128)(2,1)}), bf16[2048,1024]{1,0:T(8,128)(2,1)}) %all-gather.9.cloned.1.call-update) | async-done | bytes 4194320 | tf_op jit(solution)/shard_map/all_gather | solution.py:169
  46.1 6.2 %copy.28 = bf16[512,4,1024]{0,2,1:T(8,128)(2,1)} copy(bf16[512,4,1024]{2,0,1:T(8,128)(2,1)} %bitcast.126) | data formatting | bytes 8388608 | tf_op jit(solution)/shard_map/reshape | solution.py:169
  52.3 4.9 %convolution_convert_fusion.1 = bf16[512,256]{1,0:T(8,128)(2,1)} fusion(bf16[512,4096]{0,1:T(8,128)(2,1)} %bitcast.120, bf16[4096,256]{1,0:T(8,128)(2,1)} %param.25), kind=kOutput, calls=%fused_computation.34 | convolution fusion | flops 1073872896 | bytes 6553600 | tf_op jit(solution)/shard_map/dot_general | solution.py:171
  58.8 3.7 %convolution_convert_fusion.4 = bf16[512,128]{0,1:T(8,128)(2,1)S(1)} fusion(bf16[512,4096]{0,1:T(8,128)(2,1)} %bitcast.121, bf16[4096,128]{1,0:T(8,128)(2,1)} %param.21), kind=kOutput, calls=%fused_computation.37 | convolution fusion | flops 536936448 | bytes 5373952 | tf_op jit(solution)/shard_map/dot_general | solution.py:171
  66.6 5.2 %collective-permute-start = (bf16[128,256]{0,1:T(8,128)(2,1)}, bf16[128,256]{0,1:T(8,128)(2,1)}, u32[]{:S(2)}, u32[]{:S(2)}) collective-permute-start(bf16[128,256]{0,1:T(8,128)(2,1)} %bitcast.11), channel_id=1, source_target_pairs={{0,4},{4,8},{8,12},{12,16},{16,20},{20,24},{24,28},{1,5},{5,9},{9,... | collective-permute-start | bytes 196616 | tf_op jit(solution)/shard_map/ppermute | solution.py:19
  71.7 2.0 convolution_convert_fusion.2
  73.7 5.8 %convolution_convert_fusion = bf16[512,384]{0,1:T(8,128)(2,1)} fusion(bf16[512,4096]{0,1:T(8,128)(2,1)} %bitcast.122, bf16[4096,384]{1,0:T(8,128)(2,1)} %param.19), kind=kOutput, calls=%fused_computation.33 | convolution fusion | flops 1610809344 | bytes 7733248 | tf_op jit(solution)/shard_map/dot_general | solution.py:171
  79.8 4.9 %convolution_convert_fusion.3 = bf16[512,256]{1,0:T(8,128)(2,1)} fusion(bf16[512,4096]{0,1:T(8,128)(2,1)} %bitcast.123, bf16[4096,256]{1,0:T(8,128)(2,1)} %param.23), kind=kOutput, calls=%fused_computation.36 | convolution fusion | flops 1073872896 | bytes 6553600 | tf_op jit(solution)/shard_map/dot_general | solution.py:171
  85.7 1.7 fusion.23
  87.4 2.3 fusion.24
  89.8 2.7 fusion.40
  92.5 5.6 %fusion.52 = f32[512,4096]{1,0:T(8,128)} fusion(bf16[512,384]{0,1:T(8,128)(2,1)S(1)} %bitcast.134, bf16[384,4096]{1,0:T(8,128)(2,1)S(1)} %copy-done), kind=kOutput, calls=%fused_computation.68 | convolution fusion | flops 1610612736 | bytes 11927552 | tf_op jit(solution)/shard_map/dot_general | solution.py:177
  98.1 9.4 %all-gather.7.cloned.1.call-done = bf16[4096,256]{1,0:T(8,128)(2,1)} async-done(((bf16[512,256]{1,0:T(8,128)(2,1)}), bf16[4096,256]{1,0:T(8,128)(2,1)}) %all-gather.7.cloned.1.call-update) | async-done | bytes 2097168 | tf_op jit(solution)/shard_map/all_gather | solution.py:126
  107.5 49.8 %all-gather.5.cloned.1.call-done = bf16[4096,256]{1,0:T(8,128)(2,1)} async-done(((bf16[512,256]{1,0:T(8,128)(2,1)}), bf16[4096,256]{1,0:T(8,128)(2,1)}) %all-gather.5.cloned.1.call-update) | async-done | bytes 2097168 | tf_op jit(solution)/shard_map/all_gather | solution.py:125
  157.2 89.2 %conditional.1 = (f32[4,2,512]{2,1,0:T(2,128)}, f32[4,2,512,64]{2,3,1,0:T(8,128)}) conditional(s32[]{:T(128)} %convert_element_type.55, () %tuple.34, (s32[512]{0:T(512)S(1)}, bf16[512,256]{1,0:T(8,128)(2,1)S(1)}, bf16[4096,256]{1,0:T(8,128)(2,1)}, bf16[4096,256]{1,0:T(8,128)(2,1)}, s32[]{:T(128)}, /*index=5*/s32[]{:T(128)}) %tuple.80), branch_computations={%region_3.4_spmd, %region_4.9_spmd.clone} | conditional | flops 859970048 | bytes 132364824 | solution.py:127
  158.7 4.1 %copy.44 = bf16[4096,256]{0,1:T(8,128)(2,1)} copy(bf16[4096,256]{1,0:T(8,128)(2,1)} %get-tuple-element.257) | data formatting | bytes 4194304 | tf_op jit(solution)/shard_map
  162.8 2.9 copy.43
  167.5 79.0 %while.37 = (s32[]{:T(128)}, f32[4,2,512]{2,1,0:T(2,128)S(1)}, f32[4,2,512]{2,1,0:T(2,128)}, f32[4,2,512,64]{2,3,1,0:T(8,128)}, s32[]{:T(128)}, /*index=5*/s32[]...) while((s32[]{:T(128)}, f32[4,2,512]{2,1,0:T(2,128)S(1)}, ...), condition=%wide.region_8.8_spmd, body=%wide.region_5.7_spmd.sunk | while | flops 859969536 | bytes 122368224 | solution.py:109
  168.1 2.7 fusion.82
  170.9 4.9 %fusion.83 = f32[4,2,128]{2,1,0:T(2,128)S(1)} fusion(f32[4,2,128,4096]{3,2,1,0:T(8,128)S(1)} %get-tuple-element.364, f32[4,2,128]{2,1,0:T(2,128)S(1)} %get-tuple-element.365, pred[4096]{0:T(1024)(128)(4,1)S(1)} %iota_compare_fusion.2), kind=kLoop, calls=%fused_computation.4.clone.1 | loop fusion | flops 20970496 | bytes 16789504 | tf_op jit(solution)/shard_map/cond/branch_1_fun/while/body/while/body/eval_jaxpr/reduce_sum | solution.py:93
  177.9 9.3 %fusion.84 = f32[4,2,512,64]{2,3,1,0:T(8,128)} fusion(f32[4,2,512,64]{2,3,1,0:T(8,128)} %get-tuple-element.384, s32[]{:T(128)S(6)} %select_n.128, bf16[4096,4,64]{0,2,1:T(8,128)(2,1)} %get-tuple-element.402, f32[4,2,128,4096]{3,2,1,0:T(8,128)} %copy-done.2, f32[4,2,128]{2,1,0:T(2,128)S(1)} %get-tuple-element.365, ...), kind=kOutput, calls=%fused_computation.9.clone.1 | convolution fusion | flops 557973504 | bytes 19410948 | tf_op jit(solution)/shard_map/cond/branch_1_fun/while/body/while/body/eval_jaxpr/hmqk,khd->hmqd/dot_general | solution.py:94
  187.9 2.7 fusion.82
  190.7 4.9 %fusion.83 = f32[4,2,128]{2,1,0:T(2,128)S(1)} fusion(f32[4,2,128,4096]{3,2,1,0:T(8,128)S(1)} %get-tuple-element.364, f32[4,2,128]{2,1,0:T(2,128)S(1)} %get-tuple-element.365, pred[4096]{0:T(1024)(128)(4,1)S(1)} %iota_compare_fusion.2), kind=kLoop, calls=%fused_computation.4.clone.1 | loop fusion | flops 20970496 | bytes 16789504 | tf_op jit(solution)/shard_map/cond/branch_1_fun/while/body/while/body/eval_jaxpr/reduce_sum | solution.py:93
  197.6 9.3 %fusion.84 = f32[4,2,512,64]{2,3,1,0:T(8,128)} fusion(f32[4,2,512,64]{2,3,1,0:T(8,128)} %get-tuple-element.384, s32[]{:T(128)S(6)} %select_n.128, bf16[4096,4,64]{0,2,1:T(8,128)(2,1)} %get-tuple-element.402, f32[4,2,128,4096]{3,2,1,0:T(8,128)} %copy-done.2, f32[4,2,128]{2,1,0:T(2,128)S(1)} %get-tuple-element.365, ...), kind=kOutput, calls=%fused_computation.9.clone.1 | convolution fusion | flops 557973504 | bytes 19410948 | tf_op jit(solution)/shard_map/cond/branch_1_fun/while/body/while/body/eval_jaxpr/hmqk,khd->hmqd/dot_general | solution.py:94
  207.6 2.7 fusion.82
  210.4 4.9 %fusion.83 = f32[4,2,128]{2,1,0:T(2,128)S(1)} fusion(f32[4,2,128,4096]{3,2,1,0:T(8,128)S(1)} %get-tuple-element.364, f32[4,2,128]{2,1,0:T(2,128)S(1)} %get-tuple-element.365, pred[4096]{0:T(1024)(128)(4,1)S(1)} %iota_compare_fusion.2), kind=kLoop, calls=%fused_computation.4.clone.1 | loop fusion | flops 20970496 | bytes 16789504 | tf_op jit(solution)/shard_map/cond/branch_1_fun/while/body/while/body/eval_jaxpr/reduce_sum | solution.py:93
  217.4 9.3 %fusion.84 = f32[4,2,512,64]{2,3,1,0:T(8,128)} fusion(f32[4,2,512,64]{2,3,1,0:T(8,128)} %get-tuple-element.384, s32[]{:T(128)S(6)} %select_n.128, bf16[4096,4,64]{0,2,1:T(8,128)(2,1)} %get-tuple-element.402, f32[4,2,128,4096]{3,2,1,0:T(8,128)} %copy-done.2, f32[4,2,128]{2,1,0:T(2,128)S(1)} %get-tuple-element.365, ...), kind=kOutput, calls=%fused_computation.9.clone.1 | convolution fusion | flops 557973504 | bytes 19410948 | tf_op jit(solution)/shard_map/cond/branch_1_fun/while/body/while/body/eval_jaxpr/hmqk,khd->hmqd/dot_general | solution.py:94
  227.3 2.7 fusion.82
  230.1 4.9 %fusion.83 = f32[4,2,128]{2,1,0:T(2,128)S(1)} fusion(f32[4,2,128,4096]{3,2,1,0:T(8,128)S(1)} %get-tuple-element.364, f32[4,2,128]{2,1,0:T(2,128)S(1)} %get-tuple-element.365, pred[4096]{0:T(1024)(128)(4,1)S(1)} %iota_compare_fusion.2), kind=kLoop, calls=%fused_computation.4.clone.1 | loop fusion | flops 20970496 | bytes 16789504 | tf_op jit(solution)/shard_map/cond/branch_1_fun/while/body/while/body/eval_jaxpr/reduce_sum | solution.py:93
  237.1 9.3 %fusion.84 = f32[4,2,512,64]{2,3,1,0:T(8,128)} fusion(f32[4,2,512,64]{2,3,1,0:T(8,128)} %get-tuple-element.384, s32[]{:T(128)S(6)} %select_n.128, bf16[4096,4,64]{0,2,1:T(8,128)(2,1)} %get-tuple-element.402, f32[4,2,128,4096]{3,2,1,0:T(8,128)} %copy-done.2, f32[4,2,128]{2,1,0:T(2,128)S(1)} %get-tuple-element.365, ...), kind=kOutput, calls=%fused_computation.9.clone.1 | convolution fusion | flops 557973504 | bytes 19410948 | tf_op jit(solution)/shard_map/cond/branch_1_fun/while/body/while/body/eval_jaxpr/hmqk,khd->hmqd/dot_general | solution.py:94
  249.1 6.8 %add_convert_fusion = bf16[512,4096]{1,0:T(8,128)(2,1)} fusion(f32[512,4096]{1,0:T(8,128)} %fusion.52, bf16[512,256]{0,1:T(8,128)(2,1)S(1)} %bitcast.129, bf16[256,4096]{1,0:T(8,128)(2,1)S(1)} %copy-done.4), kind=kOutput, calls=%fused_computation.23 | convolution fusion | flops 1077936128 | bytes 14942208 | tf_op jit(solution)/shard_map/dot_general | solution.py:179
  256.0 43.2 %reduce-scatter.2.cloned.1.call-done = bf16[128,4096]{1,0:T(8,128)(2,1)} async-done(((bf16[512,4096]{1,0:T(8,128)(2,1)}), bf16[128,4096]{1,0:T(8,128)(2,1)}) %reduce-scatter.2.cloned.1.call-update) | async-done | bytes 1048592 | tf_op jit(solution)/shard_map/reduce_scatter | solution.py:178
  (92 shorter events, 23.3 us)
Async XLA Ops:
  6.5 85.9 %copy-start = (bf16[384,4096]{1,0:T(8,128)(2,1)S(1)}, bf16[384,4096]{1,0:T(8,128)(2,1)}, u32[]{:S(2)}) copy-start(bf16[384,4096]{1,0:T(8,128)(2,1)} %param.28) | copy-start | bytes 9437188
  6.5 39.6 %all-gather.9.cloned.1.call-start = ((), (), s32[]{:S(2)}) async-start(), calls=%async_computation.4 | async-start | bytes 5242880 | tf_op jit(solution)/shard_map/all_gather | solution.py:169
  7.3 100.2 %all-gather.7.cloned.1.call-start = ((), (), s32[]{:S(2)}) async-start(), calls=%async_computation.2 | async-start | bytes 2359296 | tf_op jit(solution)/shard_map/all_gather | solution.py:126
  52.3 5.6 %copy-start.15 = (f32[6]{0:T(128)S(1)}, f32[6]{0:T(128)}, u32[]{:S(2)}) copy-start(f32[6]{0:T(128)} %param.22) | copy-start | bytes 76
  57.2 100.0 %all-gather.5.cloned.1.call-start = ((), (), s32[]{:S(2)}) async-start(), calls=%async_computation.1 | async-start | bytes 2359296 | tf_op jit(solution)/shard_map/all_gather | solution.py:125
  58.0 4.5 %copy-start.3 = (bf16[512,4,1024]{0,2,1:T(8,128)(2,1)S(1)}, bf16[512,4,1024]{0,2,1:T(8,128)(2,1)}, u32[]{:S(2)}) copy-start(bf16[512,4,1024]{0,2,1:T(8,128)(2,1)} %copy.28) | copy-start | bytes 12582916
  58.0 4.5 %copy-start.14 = (bf16[4096,128]{1,0:T(8,128)(2,1)S(1)}, bf16[4096,128]{1,0:T(8,128)(2,1)}, u32[]{:S(2)}) copy-start(bf16[4096,128]{1,0:T(8,128)(2,1)} %param.20) | copy-start | bytes 3145732
  62.6 0.8 copy-start.5
  62.6 9.2 %copy-start.13 = (bf16[4096,256]{1,0:T(8,128)(2,1)S(1)}, bf16[4096,256]{1,0:T(8,128)(2,1)}, u32[]{:S(2)}) copy-start(bf16[4096,256]{1,0:T(8,128)(2,1)} %param.24) | copy-start | bytes 6291460
  63.4 0.6 copy-start.7
  65.3 19.5 %collective-permute-start.1 = (bf16[128,256]{0,1:T(8,128)(2,1)}, bf16[128,256]{0,1:T(8,128)(2,1)}, u32[]{:S(2)}, u32[]{:S(2)}) collective-permute-start(bf16[128,256]{0,1:T(8,128)(2,1)} %bitcast.13), channel_id=1, source_target_pairs={{4,0},{8,4},{12,8},{16,12},{20,16},{24,20},{28,24},{5,1},{9,5},{13... | collective-permute-start | bytes 196616 | tf_op jit(solution)/shard_map/ppermute | solution.py:22
  66.6 18.2 %collective-permute-start = (bf16[128,256]{0,1:T(8,128)(2,1)}, bf16[128,256]{0,1:T(8,128)(2,1)}, u32[]{:S(2)}, u32[]{:S(2)}) collective-permute-start(bf16[128,256]{0,1:T(8,128)(2,1)} %bitcast.11), channel_id=1, source_target_pairs={{0,4},{4,8},{8,12},{12,16},{16,20},{20,24},{24,28},{1,5},{5,9},{9,... | collective-permute-start | bytes 196616 | tf_op jit(solution)/shard_map/ppermute | solution.py:19
  79.5 219.7 %reduce-scatter.2.cloned.1.call-start = ((), (), s32[]{:S(2)}) async-start(), calls=%async_computation.3 | async-start | bytes 5242880 | tf_op jit(solution)/shard_map/reduce_scatter | solution.py:178
  79.8 5.0 %copy-start.6 = (bf16[512,128]{0,1:T(8,128)(2,1)S(1)}, bf16[512,128]{0,1:T(8,128)(2,1)}, u32[]{:S(2)}) copy-start(bf16[512,128]{0,1:T(8,128)(2,1)} %copy-done.5) | copy-start | bytes 393220
  79.8 5.0 %copy-start.8 = (bf16[512,128]{0,1:T(8,128)(2,1)S(1)}, bf16[512,128]{0,1:T(8,128)(2,1)}, u32[]{:S(2)}) copy-start(bf16[512,128]{0,1:T(8,128)(2,1)} %copy-done.7) | copy-start | bytes 393220
  79.8 5.9 %copy-start.9 = (bf16[512,384]{0,1:T(8,128)(2,1)S(1)}, bf16[512,384]{0,1:T(8,128)(2,1)}, u32[]{:S(2)}) copy-start(bf16[512,384]{0,1:T(8,128)(2,1)} %convolution_convert_fusion) | copy-start | bytes 1179652
  92.5 64.8 %copy-start.10 = (bf16[512,256]{1,0:T(8,128)(2,1)S(1)}, bf16[512,256]{1,0:T(8,128)(2,1)}, u32[]{:S(2)}) copy-start(bf16[512,256]{1,0:T(8,128)(2,1)} %convolution_convert_fusion.3) | copy-start | bytes 786436
  157.2 91.4 %copy-start.11 = (f32[4]{0:T(128)S(1)}, f32[4]{0:T(128)}, u32[]{:S(2)}) copy-start(f32[4]{0:T(128)} %param.26) | copy-start | bytes 52
  157.2 91.7 %copy-start.12 = (f32[64]{0:T(128)S(1)}, f32[64]{0:T(128)}, u32[]{:S(2)}) copy-start(f32[64]{0:T(128)} %param.27) | copy-start | bytes 772
  170.9 5.7 %copy-start.2 = (f32[4,2,128,4096]{3,2,1,0:T(8,128)}, f32[4,2,128,4096]{3,2,1,0:T(8,128)S(1)}, u32[]{:S(2)}) copy-start(f32[4,2,128,4096]{3,2,1,0:T(8,128)S(1)} %get-tuple-element.364) | copy-start | bytes 50331652 | tf_op jit(solution)/shard_map/cond/branch_1_fun/while
  190.6 5.7 %copy-start.2 = (f32[4,2,128,4096]{3,2,1,0:T(8,128)}, f32[4,2,128,4096]{3,2,1,0:T(8,128)S(1)}, u32[]{:S(2)}) copy-start(f32[4,2,128,4096]{3,2,1,0:T(8,128)S(1)} %get-tuple-element.364) | copy-start | bytes 50331652 | tf_op jit(solution)/shard_map/cond/branch_1_fun/while
  210.3 5.7 %copy-start.2 = (f32[4,2,128,4096]{3,2,1,0:T(8,128)}, f32[4,2,128,4096]{3,2,1,0:T(8,128)S(1)}, u32[]{:S(2)}) copy-start(f32[4,2,128,4096]{3,2,1,0:T(8,128)S(1)} %get-tuple-element.364) | copy-start | bytes 50331652 | tf_op jit(solution)/shard_map/cond/branch_1_fun/while
  230.1 5.7 %copy-start.2 = (f32[4,2,128,4096]{3,2,1,0:T(8,128)}, f32[4,2,128,4096]{3,2,1,0:T(8,128)S(1)}, u32[]{:S(2)}) copy-start(f32[4,2,128,4096]{3,2,1,0:T(8,128)S(1)} %get-tuple-element.364) | copy-start | bytes 50331652 | tf_op jit(solution)/shard_map/cond/branch_1_fun/while
  246.4 2.7 copy-start.4
  249.1 50.1 %copy-start.1 = (bf16[384,4096]{1,0:T(8,128)(2,1)S(1)}, bf16[384,4096]{1,0:T(8,128)(2,1)}, u32[]{:S(2)}) copy-start(bf16[384,4096]{1,0:T(8,128)(2,1)} %param.28) | copy-start | bytes 9437188
Sparse Core Ops, SparseCore 0:
  8.9 37.1 all-gather.8
  57.3 50.0 all-gather.6
  109.6 47.6 all-gather.4
  256.1 43.0 reduce-scatter.1
